TPU v7x, 128 devices: a whole 4x4x4 slice. The times are simulated.
128 devices in a mesh: sp: 16 (over z, x), tp: 8 (over y, core).
Axes of the slice: x: 4, y: 4, z: 4, core: 2. Of those that a mesh axis runs over, the one named last changes fastest.
Arguments:
- queries: bfloat16 [8192, 3072], P('sp', 'tp'), may hold values from -6 to 6
- latent: bfloat16 [8192, 1024], P('sp'), may hold values from -6 to 6
- rope_key: bfloat16 [8192, 64], P('sp'), may hold values from -6 to 6
- key_weight: bfloat16 [1024, 2048], P(None, 'tp'), as said below
- value_weight: bfloat16 [1024, 2048], P(None, 'tp'), as said below
- log_sums: float32 [16, 8192], P('tp', 'sp'), as said below
- attn_out: bfloat16 [8192, 2048], P('sp', 'tp'), as said below
- out_grad: bfloat16 [8192, 2048], P('sp', 'tp'), may hold values from -6 to 6
Outputs:
- d_queries: bfloat16 [8192, 3072], P('sp', 'tp')
- d_latent: float32 [8192, 1024], P('sp')
- d_rope: float32 [8192, 64], P('sp')
- d_value_weight: float32 [1024, 2048], P('sp', 'tp')
Inputs may be any that keep to these rules, and one draw needn't show every extreme that they name: `key_weight`: independent entries of order one multiplied by 1024^(-1/2). `value_weight`: independent entries of order one multiplied by 1024^(-1/2). log_sums[h, i] is the logarithm of the sum over j <= i of exp(scores[h, i, j]) of the forward pass. attn_out is the forward pass output: head h of row i is the sum over j <= i of exp(scores - log_sums) rounded to bfloat16, times head h of values row j, rounded to bfloat16.
All inputs are finite; a program needn't handle non-finite values.
Results may differ from a plain program's by a relative error of at most 0.018.
Values may be sent and summed in bfloat16 or wider, within the bound.
A program may use at most 192 MiB of HBM per device.

v0:
```python
import jax
import jax.numpy as jnp
from jax import lax
from jax.experimental import pallas as pl
from jax.experimental.pallas import tpu as pltpu
from jax.sharding import PartitionSpec as P

NOPE = 128
ROPE = 64
HEAD = NOPE + ROPE
VDIM = 128
ROWS = 512
LATENT = 1024
WIDE = 1152
SCALE = HEAD**-0.5
LOG2E = 1.4426950408889634
BF16 = jnp.bfloat16
F32 = jnp.float32
MESH = pl.DeviceIdType.MESH
NT = (((1,), (1,)), ((), ()))

LSE_AT, GRAD_AT, PACK = 192, 208, 336
ONES_AT, VALUE_AT, KEY_PACK = 192, 224, 352


def dot(a, b):
    return jnp.dot(a, b, preferred_element_type=F32)


def dot_nt(a, b):
    return lax.dot_general(a, b, NT, preferred_element_type=F32)


def in_three(row):
    high = row.astype(BF16).astype(F32)
    middle = (row - high).astype(BF16).astype(F32)
    return high, middle, row - high - middle


def six_rows(first, second):
    at = lax.broadcasted_iota(jnp.int32, (16, first.shape[1]), 0)
    rows = jnp.zeros(at.shape, F32)
    for i, part in enumerate(in_three(first) + in_three(second)):
        rows = jnp.where(at == i, part, rows)
    return rows.astype(BF16)


def ones_rows(first):
    at = lax.broadcasted_iota(jnp.int32, (16, ROWS), 0)
    return jnp.where((at >= first) & (at < first + 3), 1.0, 0.0).astype(BF16)


def kernel(
    q_hbm, lat_hbm, rope_hbm, kw_hbm, vw_hbm, lse_hbm, ao_hbm, go_hbm,
    ag, dq_out, dw_out,
    q, lat, rope, kw, vw, lse, ao, go,
    qb, pk, kts, vts, kv, kaug, vaug, dk, dv, dq,
    dqs, dqr, xs, rel, fin, dqh, dqf, gs, gf, kvb, latt,
    part, half, hr, ys, yr, dws, dwr, dws2, dwr2,
    s_in, s_pk, s_kt, s_v, r_q, r_kt, r_v, s_fw, s_d, r_d, s_x, r_rel, r_fin, s_h, r_h, s_g, r_g,
    s_l, r_l, s_y, r_y, s_ag, s_agp, r_ag, s_w, r_w, s_w2, r_w2,
):
    sp, tp = lax.axis_index("sp"), lax.axis_index("tp")
    z, x, y, c = sp // 4, sp % 4, tp // 2, tp % 2
    core_of_z = ((z + 1) // 2) % 2
    slot_of_z = z // 2
    partner = (sp, 2 * y + 1 - c)

    def key_z(core, slot):
        return core + slot * (3 - 2 * core)

    def x_peer(j):
        return (4 * z + (x + j) % 4, tp)

    def z_peer(j):
        return (4 * ((z + j) % 4) + x, tp)

    def y_peer(j):
        return (sp, 2 * ((y + j) % 4) + c)

    def remote(src, dst, send, recv, to):
        return pltpu.make_async_remote_copy(
            src_ref=src, dst_ref=dst, send_sem=send, recv_sem=recv, device_id=to, device_id_type=MESH
        )

    def arrived(ref, recv, name="wait"):
        with jax.named_scope(name):
            remote(ref, ref, s_l.at[0], recv, partner).wait_recv()

    barrier = pltpu.get_barrier_semaphore()
    peers = [partner]
    for j in (1, 2, 3):
        peers += [x_peer(j), y_peer(j)]
        peers += [(4 * ((z + j) % 4) + x, 2 * y + core) for core in (0, 1)]
    for peer in peers:
        pl.semaphore_signal(barrier, inc=1, device_id=peer, device_id_type=MESH)

    pairs = [(q_hbm, q), (go_hbm, go), (ao_hbm, ao), (lse_hbm, lse), (lat_hbm, lat), (kw_hbm, kw), (vw_hbm, vw), (rope_hbm, rope)]
    loads = [pltpu.make_async_copy(src, dst, s_in.at[i]) for i, (src, dst) in enumerate(pairs)]
    for load in loads:
        load.start()

    dk[...] = jnp.zeros_like(dk)
    dv[...] = jnp.zeros_like(dv)
    for s in (0, 1):
        kv[s, ONES_AT : ONES_AT + 16] = ones_rows(0)
        kv[s, ONES_AT + 16 : VALUE_AT] = ones_rows(3)

    with jax.named_scope("inputs"):
        for load in loads:
            load.wait()
    with jax.named_scope("barrier"):
        pl.semaphore_wait(barrier, len(peers))

    def to_head(e, src, dst, send, recv):
        head_z = 2 * c + e
        own = (head_z == z) & (core_of_z == c)
        copy = remote(src, dst, send, recv, (4 * head_z + x, 2 * y + core_of_z))
        return own, copy, pltpu.make_async_copy(src, dst, recv)

    def start_to_head(args):
        own, copy, local = to_head(*args)

        @pl.when(own)
        def _():
            local.start()

        @pl.when(jnp.logical_not(own))
        def _():
            copy.start()

    def sent_to_head(args):
        own, copy, _ = to_head(*args)

        @pl.when(jnp.logical_not(own))
        def _():
            copy.wait_send()

    pack_args = [(e, pk.at[e], qb.at[sp], s_pk.at[e], r_q.at[sp]) for e in (0, 1)]
    key_args = [
        (e, kts.at[e], kv.at[slot_of_z, pl.ds(0, HEAD)], s_kt.at[e], r_kt.at[slot_of_z]) for e in (0, 1)
    ]
    value_args = [
        (e, vts.at[e], kv.at[slot_of_z, pl.ds(VALUE_AT, VDIM)], s_v.at[e], r_v.at[slot_of_z]) for e in (0, 1)
    ]

    def send_queries():
        qt = q[...].T
        got = go[...].T
        aot = ao[...].T
        for e in (0, 1):
            grad = got[e * VDIM : (e + 1) * VDIM]
            delta = jnp.sum(
                grad.astype(F32) * aot[e * VDIM : (e + 1) * VDIM].astype(F32), axis=0, keepdims=True
            )
            pk[e, 0:LSE_AT] = qt[e * HEAD : (e + 1) * HEAD]
            pk[e, LSE_AT:GRAD_AT] = six_rows(lse[e : e + 1, :] * (-1.0 / SCALE), -delta)
            pk[e, GRAD_AT:PACK] = grad
            start_to_head(pack_args[e])

    def send_keys():
        keys = dot(lat[...], kw[...]).astype(BF16).T
        for e in (0, 1):
            kts[e, 0:NOPE] = keys[e * NOPE : (e + 1) * NOPE]
            kts[e, NOPE:HEAD] = rope[...]
            start_to_head(key_args[e])
        values = dot(lat[...], vw[...]).astype(BF16).T
        for e in (0, 1):
            vts[e] = values[e * VDIM : (e + 1) * VDIM]
            start_to_head(value_args[e])

    @pl.when(z < 2)
    def _():
        send_keys()
        send_queries()

    @pl.when(z >= 2)
    def _():
        send_queries()
        send_keys()

    def zero(b, _):
        dq[b] = jnp.zeros((HEAD, ROWS), F32)
        return 0

    lax.fori_loop(0, 16, zero, 0)

    def step(t):
        near = t < 4
        far = t >= 12
        mid = jnp.logical_not(near | far)
        pair = t % 2
        slot = 1 - jnp.where(mid, (t - 4) // 4, (t % 4) // 2)
        other = jnp.where(mid, ((t - 4) // 2) % 2, pair)
        dx = jnp.where(near, 0, jnp.where(far, 2, jnp.where(pair == 0, 3, 1)))
        core = jnp.where(other == 0, c, 1 - c)
        block = 4 * key_z(core, slot) + (x + dx) % 4
        return block, dx, other, slot

    def forwards(t):
        b, dx, other, slot = step(t)
        mine = other == 0
        plus = mine & ((dx == 0) | ((dx == 3) & (slot == 0)))
        minus = mine & ((dx == 0) | ((dx == 1) & (slot == 1)))
        return [
            (plus, remote(qb.at[b], qb.at[b], s_fw.at[0, b], r_q.at[b], x_peer(1))),
            (minus, remote(qb.at[b], qb.at[b], s_fw.at[1, b], r_q.at[b], x_peer(3))),
            (mine, remote(qb.at[b], qb.at[b], s_fw.at[2, b], r_q.at[b], partner)),
        ]

    def take(t):
        b = step(t)[0]
        arrived(qb.at[b], r_q.at[b], "wait_query")
        for holds, copy in forwards(t):

            @pl.when(holds)
            def _():
                copy.start()

    def tile(b, s, masked):
        raw = dot(kaug[s], qb[b, 0:GRAD_AT]) * (SCALE * LOG2E)
        if masked:
            key_row = lax.broadcasted_iota(jnp.int32, (ROWS, ROWS), 0)
            query_row = lax.broadcasted_iota(jnp.int32, (ROWS, ROWS), 1)
            raw = jnp.where(key_row <= query_row, raw, -1e30)
        probs = jnp.exp2(raw)
        diff = dot(vaug[s], qb[b, LSE_AT:PACK])
        grads = (probs * diff).astype(BF16)
        dv[s] += dot_nt(probs.astype(BF16), qb[b, GRAD_AT:PACK])
        dk[s] += dot_nt(grads, qb[b, 0:LSE_AT])
        dq[b] += dot(kv[s, 0:HEAD], grads)

    def to_partner(i):
        return remote(dqs.at[i], dqr.at[i], s_d.at[i], r_d.at[i], partner)

    def share(t):
        b, dx, other, slot = step(t)

        @pl.when(other == 1)
        def _():
            i = 2 * dx + slot
            dqs[i] = dq[b].astype(BF16)
            to_partner(i).start()

    def own_block(s):
        return 4 * key_z(c, s) + x

    def take_keys(s):
        arrived(kv.at[s, pl.ds(0, HEAD)], r_kt.at[s], "wait_keys")
        arrived(kv.at[s, pl.ds(VALUE_AT, VDIM)], r_v.at[s], "wait_values")
        kaug[s] = kv[s, 0:GRAD_AT].T
        vaug[s] = kv[s, GRAD_AT:KEY_PACK].T

    def tiles(t):
        b = step(t)[0]

        def pair(s, _):
            @pl.when(b > own_block(s))
            def _():
                tile(b, s, False)

            return 0

        with jax.named_scope("pair"):
            lax.fori_loop(0, 2, pair, 0)

    def early(t, _):
        take(t)
        with jax.named_scope("early"):
            tile(step(t)[0], 0, False)
        return 0

    def diagonal(s, _):
        tile(own_block(s), s, True)
        return 0

    def later(t, _):
        take(t)
        tiles(t)
        share(t)
        return 0

    take_keys(0)
    lax.fori_loop(0, 2, early, 0)
    take(2)
    take_keys(1)
    with jax.named_scope("diagonal"):
        lax.fori_loop(0, 2, diagonal, 0)

    @pl.when(step(1)[0] > own_block(1))
    def _():
        tile(step(1)[0], 1, False)

    share(1)
    lax.fori_loop(3, 16, later, 0)

    def to_owner(s, src, dst, send, recv):
        token_z = key_z(c, s)
        own = (token_z == z) & (z // 2 == c)
        copy = remote(src, dst, send, recv, (4 * token_z + x, 2 * y + z // 2))
        return own, copy, pltpu.make_async_copy(src, dst, recv)

    def start_to_owner(args):
        own, copy, local = to_owner(*args)

        @pl.when(own)
        def _():
            local.start()

        @pl.when(jnp.logical_not(own))
        def _():
            copy.start()

    def sent_to_owner(args):
        own, copy, _ = to_owner(*args)

        @pl.when(jnp.logical_not(own))
        def _():
            copy.wait_send()

    e_mine = z % 2
    back = []
    for s in (0, 1):
        gs[s, 0:ROWS] = (dk[s, :, 0:NOPE] * SCALE).astype(BF16)
        gs[s, ROWS : 2 * ROWS] = dv[s].astype(BF16)
        rope_part = (dk[s, :, NOPE:HEAD] * SCALE).astype(BF16)
        gs[s, 2 * ROWS : 2 * ROWS + 256] = jnp.concatenate([rope_part[0:256], rope_part[256:512]], axis=1)
        args = (s, gs.at[s], gf.at[e_mine], s_g.at[s], r_g.at[e_mine])
        start_to_owner(args)
        back.append(args)

    def add_share(dx, s):
        i = 2 * dx + s
        arrived(dqr.at[i], r_d.at[i], "wait_share")
        b = 4 * key_z(c, s) + (x + dx) % 4
        return dq[b] + dqr[i].astype(F32)

    returned = []

    def send_x(i, value, dst, recv, to):
        xs[i] = value.astype(BF16)
        copy = remote(xs.at[i], dst, s_x.at[i], recv, to)
        copy.start()
        returned.append(copy)

    send_x(0, add_share(2, 0), rel.at[0], r_rel.at[0], x_peer(3))
    send_x(1, add_share(2, 1), rel.at[1], r_rel.at[1], x_peer(1))
    send_x(2, add_share(3, 1), fin.at[1, 1], r_fin.at[1, 1], x_peer(3))
    send_x(3, add_share(1, 0), fin.at[0, 0], r_fin.at[0, 0], x_peer(1))

    def relay_queries():
        via_minus, via_plus = add_share(3, 0), add_share(1, 1)
        arrived(rel.at[0], r_rel.at[0], "wait_relay")
        send_x(4, via_minus + rel[0].astype(F32), fin.at[1, 0], r_fin.at[1, 0], x_peer(3))
        arrived(rel.at[1], r_rel.at[1], "wait_relay")
        send_x(5, via_plus + rel[1].astype(F32), fin.at[0, 1], r_fin.at[0, 1], x_peer(1))

    latt[...] = lat[...].T

    for e in (0, 1):
        arrived(gf.at[e], r_g.at[e], "wait_grads")
        kvb[:, e * NOPE : (e + 1) * NOPE] = gf[e, 0:ROWS]
        kvb[:, 256 + e * VDIM : 256 + (e + 1) * VDIM] = gf[e, ROWS : 2 * ROWS]

    both_ropes = gf[0, 2 * ROWS : 2 * ROWS + 256].astype(F32) + gf[1, 2 * ROWS : 2 * ROWS + 256].astype(F32)

    def latent_rows(which):
        rows = pl.ds(pl.multiple_of(256 * which, 256), 256)
        grads = dot_nt(kvb[rows, 0:256], kw[...]) + dot_nt(kvb[rows, 256:512], vw[...])
        ropes = jnp.where(which == 0, both_ropes[:, 0:ROPE], both_ropes[:, ROPE : 2 * ROPE])
        return grads, jnp.concatenate([ropes, jnp.zeros_like(ropes)], axis=1)

    grads, ropes = latent_rows(1 - c)
    half[:, 0:LATENT] = grads.astype(BF16)
    half[:, LATENT:WIDE] = ropes.astype(BF16)
    to_half = remote(half, hr, s_l.at[0], r_l.at[0], partner)
    to_half.start()
    grads, ropes = latent_rows(c)
    part[:, 0:LATENT] = grads
    part[:, LATENT:WIDE] = ropes
    arrived(hr, r_l.at[0], "wait_half")
    part[...] += hr[...].astype(F32)
    ys[...] = part[...].astype(BF16)
    sends = [to_half]
    for j in (2, 1, 3):
        yj = (y + j) % 4
        copy = remote(
            ys.at[pl.ds(pl.multiple_of(64 * yj, 64), 64)], yr.at[y], s_y.at[yj], r_y.at[y], y_peer(j)
        )
        copy.start()
        sends.append(copy)

    relay_queries()
    for b in range(16):
        dws[b % 4, b // 4] = dot(latt[64 * b : 64 * (b + 1)], kvb[:, 256:512]).astype(BF16)
    for j in (2, 1, 3):
        xj = (x + j) % 4
        copy = remote(dws.at[xj], dwr.at[x], s_w.at[xj], r_w.at[x], x_peer(j))
        copy.start()
        sends.append(copy)

    total = part[pl.ds(pl.multiple_of(64 * y, 64), 64)]
    for j in (1, 3, 2):
        yj = (y + j) % 4
        arrived(yr.at[yj], r_y.at[yj], "wait_sum")
        total += yr[yj].astype(F32)
    ag[4 * c + y] = total.astype(BF16)
    for j in (2, 1, 3):
        copy = remote(ag.at[4 * c + y], ag.at[4 * c + y], s_ag.at[j], r_ag.at[4 * c + y], y_peer(j))
        copy.start()
        sends.append(copy)
    copy = remote(ag.at[4 * c + y], ag.at[4 * c + y], s_agp.at[0], r_ag.at[4 * c + y], partner)
    copy.start()
    sends.append(copy)

    for s in (0, 1):
        home = add_share(0, s)
        for side in (0, 1):
            arrived(fin.at[side, s], r_fin.at[side, s], "wait_home")
            home += fin[side, s].astype(F32)
        dqh[s] = (home * SCALE).astype(BF16)
        args = (s, dqh.at[s], dqf.at[e_mine], s_h.at[s], r_h.at[e_mine])
        start_to_owner(args)
        back.append(args)

    weight = dws[x].astype(F32)
    for j in (1, 3, 2):
        xj = (x + j) % 4
        arrived(dwr.at[xj], r_w.at[xj], "wait_weight")
        weight += dwr[xj].astype(F32)
    dws2[...] = weight.astype(BF16)
    for j in (2, 1, 3):
        zj = (z + j) % 4
        copy = remote(dws2.at[zj], dwr2.at[z], s_w2.at[zj], r_w2.at[z], z_peer(j))
        copy.start()
        sends.append(copy)

    for j in (1, 3, 2):
        i = 4 * c + (y + j) % 4
        arrived(ag.at[i], r_ag.at[i], "wait_chunk")
        copy = remote(ag.at[i], ag.at[i], s_agp.at[j], r_ag.at[i], partner)
        copy.start()
        sends.append(copy)

    weight = dws2[z].astype(F32)
    for j in (1, 3, 2):
        zj = (z + j) % 4
        arrived(dwr2.at[zj], r_w2.at[zj], "wait_weight")
        weight += dwr2[zj].astype(F32)
    dw_out[...] = weight

    for e in (0, 1):
        arrived(dqf.at[e], r_h.at[e], "wait_queries")
    dq_out[...] = jnp.concatenate([dqf[0], dqf[1]], axis=0).T

    for j in (0, 1, 3, 2):
        i = 4 * (1 - c) + (y + j) % 4
        arrived(ag.at[i], r_ag.at[i], "wait_other_chunk")

    for args in pack_args + key_args + value_args:
        sent_to_head(args)
    for args in back:
        sent_to_owner(args)
    for copy in returned + sends:
        copy.wait_send()

    def sent(t, _):
        for holds, copy in forwards(t):

            @pl.when(holds)
            def _():
                copy.wait_send()

        b, dx, other, slot = step(t)

        @pl.when(other == 1)
        def _():
            to_partner(2 * dx + slot).wait_send()

        return 0

    lax.fori_loop(0, 16, sent, 0)


def finish(ag, dq, dw, dlat_out, drope_out, dq_out, dw_out):
    for i in range(8):
        rows = slice(64 * i, 64 * (i + 1))
        dlat_out[rows] = ag[i, :, 0:LATENT].astype(F32)
    ropes = jnp.concatenate([ag[i, :, LATENT:WIDE] for i in range(8)], axis=0).T
    drope_out[...] = ropes[0:ROPE].astype(F32)
    dq_out[...] = dq[...]
    dw_out[...] = dw[...]


def per_device(q, lat, rope, kw, vw, lse, ao, go):
    vmem = pl.BlockSpec(memory_space=pltpu.VMEM)
    anywhere = pl.BlockSpec(memory_space=pl.ANY)

    def buf(*shape, dtype=BF16):
        return pltpu.VMEM(shape, dtype)

    def sem(*shape):
        return pltpu.SemaphoreType.DMA(shape)

    scratch = [
        buf(ROWS, 2 * HEAD), buf(ROWS, LATENT), buf(ROPE, ROWS), buf(LATENT, 256), buf(LATENT, 256),
        buf(2, ROWS, dtype=F32), buf(ROWS, 256), buf(ROWS, 256),
        buf(16, PACK, ROWS), buf(2, PACK, ROWS), buf(2, HEAD, ROWS), buf(2, VDIM, ROWS),
        buf(2, KEY_PACK, ROWS), buf(2, ROWS, GRAD_AT), buf(2, ROWS, KEY_PACK - GRAD_AT),
        buf(2, ROWS, HEAD, dtype=F32), buf(2, ROWS, VDIM, dtype=F32), buf(16, HEAD, ROWS, dtype=F32),
        buf(8, HEAD, ROWS), buf(8, HEAD, ROWS), buf(6, HEAD, ROWS), buf(2, HEAD, ROWS), buf(2, 2, HEAD, ROWS),
        buf(2, HEAD, ROWS), buf(2, HEAD, ROWS), buf(2, 1280, 128), buf(2, 1280, 128), buf(ROWS, 512),
        buf(LATENT, ROWS),
        buf(256, WIDE, dtype=F32), buf(256, WIDE), buf(256, WIDE), buf(256, WIDE), buf(4, 64, WIDE),
        buf(4, 4, 64, 256), buf(4, 4, 64, 256), buf(4, 64, 256), buf(4, 64, 256),
        sem(8), sem(2), sem(2), sem(2), sem(16), sem(2), sem(2), sem(3, 16), sem(8), sem(8), sem(6), sem(2), sem(2, 2),
        sem(2), sem(2), sem(2), sem(2),
        sem(1), sem(1), sem(4), sem(4), sem(4), sem(4), sem(8), sem(4), sem(4), sem(4), sem(4),
    ]
    ag, dq, dw = pl.pallas_call(
        kernel,
        in_specs=[anywhere] * 8,
        out_specs=[vmem] * 3,
        out_shape=[
            jax.ShapeDtypeStruct((8, 64, WIDE), BF16),
            jax.ShapeDtypeStruct((ROWS, 2 * HEAD), BF16),
            jax.ShapeDtypeStruct((64, 256), F32),
        ],
        scratch_shapes=scratch,
        compiler_params=pltpu.CompilerParams(
            collective_id=0, has_side_effects=True, vmem_limit_bytes=58000 * 1024
        ),
        name="latent_attention_backward",
    )(q, lat, rope.T, kw, vw, lse, ao, go)
    dlat, drope, dq, dw = pl.pallas_call(
        finish,
        in_specs=[vmem] * 3,
        out_specs=[vmem] * 4,
        out_shape=[
            jax.ShapeDtypeStruct((ROWS, LATENT), F32),
            jax.ShapeDtypeStruct((ROPE, ROWS), F32),
            jax.ShapeDtypeStruct((ROWS, 2 * HEAD), BF16),
            jax.ShapeDtypeStruct((64, 256), F32),
        ],
        name="finish",
    )(ag, dq, dw)
    return dq, dlat, drope.T, dw


def solution(mesh):
    placed = (
        P("sp", "tp"),
        P("sp", None),
        P("sp", None),
        P(None, "tp"),
        P(None, "tp"),
        P("tp", "sp"),
        P("sp", "tp"),
        P("sp", "tp"),
    )
    return jax.shard_map(
        per_device,
        mesh=mesh,
        in_specs=placed,
        out_specs=(P("sp", "tp"), P("sp", None), P("sp", None), P("sp", "tp")),
        check_vma=False,
    )
```

profile of v0, /device:TPU:1, one launch (start us, length us, event | category | flops | bytes accessed | tf_op | source)
XLA Modules:
  0.0 83.0 jit_solution(16499602222215254920)
XLA Ops:
  0.6 79.3 %latent_attention_backward.1 = (bf16[8,64,1152]{2,1,0:T(8,128)(2,1)}, bf16[512,384]{1,0:T(8,128)(2,1)}, f32[64,256]{1,0:T(8,128)}) custom-call(bf16[512,384]{1,0:T(8,128)(2,1)} %q_hbm.1, bf16[512,1024]{1,0:T(8,128)(2,1)} %lat_hbm.1, bf16[64,512]{1,0:T(8,128)(2,1)} %bitcast.2, bf16[1024,256]{1,0:T(8,128)(2,1)} %kw_hbm.1, bf16[1024,256]{1,0:T(8,128)(2,1)} %vw_hbm.1, ...), custom_call_target="tpu_custom_call" | custom-call | tf_op jit(solution)/shard_map/latent_attention_backward/pallas_call | solution.py:520
  80.0 3.1 %finish.1 = (f32[512,1024]{1,0:T(8,128)}, f32[64,512]{1,0:T(8,128)}, bf16[512,384]{1,0:T(8,128)(2,1)}, f32[64,256]{1,0:T(8,128)}) custom-call(bf16[8,64,1152]{2,1,0:T(8,128)(2,1)} %get-tuple-element.11.ag, bf16[512,384]{1,0:T(8,128)(2,1)} %get-tuple-element.12.dq, f32[64,256]{1,0:T(8,128)} %get-tuple-element.13.dw), custom_call_target="tpu_custom_call" | custom-call | tf_op jit(solution)/shard_map/finish/pallas_call | solution.py:535
where the time goes:
time: 83.2 us; the launch traced here: 83 us
  Pallas kernels  82.4 us (99%)
    pallas_call x1, Pallas kernels, per_device(): pl.pallas_call(kernel, in_specs=[anywhere] * 8, out_specs=[vmem] * 3, out...  79.3 us
    pallas_call x1, Pallas kernels, per_device(): pl.pallas_call(finish, in_specs=[vmem] * 3, out_specs=[vmem] * 4, out_sha...  3.06 us

commit v1 on v0

v1 whole, which is shorter than its diff:
```python
import jax
import jax.numpy as jnp
from jax import lax
from jax.experimental import pallas as pl
from jax.experimental.pallas import tpu as pltpu
from jax.sharding import PartitionSpec as P

NOPE = 128
ROPE = 64
HEAD = NOPE + ROPE
VDIM = 128
ROWS = 512
LATENT = 1024
CHUNK = 64
PIECE = 160
DONE = 544
HALF = 256
SCALE = HEAD**-0.5
LOG2E = 1.4426950408889634
BF16 = jnp.bfloat16
F32 = jnp.float32
MESH = pl.DeviceIdType.MESH
NT = (((1,), (1,)), ((), ()))

LSE_AT, GRAD_AT, PACK = 192, 208, 336
ONES_AT, VALUE_AT, KEY_PACK = 192, 224, 352


def dot(a, b):
    return jnp.dot(a, b, preferred_element_type=F32)


def dot_nt(a, b):
    return lax.dot_general(a, b, NT, preferred_element_type=F32)


def in_three(row):
    high = row.astype(BF16).astype(F32)
    middle = (row - high).astype(BF16).astype(F32)
    return high, middle, row - high - middle


def six_rows(first, second):
    at = lax.broadcasted_iota(jnp.int32, (16, first.shape[1]), 0)
    rows = jnp.zeros(at.shape, F32)
    for i, part in enumerate(in_three(first) + in_three(second)):
        rows = jnp.where(at == i, part, rows)
    return rows.astype(BF16)


def ones_rows(first):
    at = lax.broadcasted_iota(jnp.int32, (16, ROWS), 0)
    return jnp.where((at >= first) & (at < first + 3), 1.0, 0.0).astype(BF16)


def kernel(
    q_hbm, lat_hbm, rope_hbm, kw_hbm, vw_hbm, lse_hbm, ao_hbm, go_hbm,
    ag_out, dq_out, dw_out,
    q, lat, rope, kw, vw, lse, ao, go,
    qb, pk, kts, vts, kv, kaug, vaug, dk, dv, dq,
    dqs, dqr, xs, rel, fin, dqh, dqf, gs, gf, lt, wt,
    dwh, dwhr, dwx, dwxr, dwz, dwf, ag, dqo, dwo,
    s_in, s_pk, s_kt, s_v, r_q, r_kt, r_v, s_fw, s_d, r_d, s_x, r_rel, r_fin, s_h, r_h, s_g, r_g,
    s_lt, r_lt, s_wt, r_wt, s_ag, r_ag, s_wh, r_wh, s_wx, r_wx, s_wz, r_wz, s_out,
):
    sp, tp = lax.axis_index("sp"), lax.axis_index("tp")
    z, x, y, c = sp // 4, sp % 4, tp // 2, tp % 2
    core_of_z = ((z + 1) // 2) % 2
    slot_of_z = z // 2
    partner = (sp, 2 * y + 1 - c)

    def key_z(core, slot):
        return core + slot * (3 - 2 * core)

    def x_peer(j):
        return (4 * z + (x + j) % 4, tp)

    def z_peer(j):
        return (4 * ((z + j) % 4) + x, tp)

    def y_peer(j):
        return (sp, 2 * ((y + j) % 4) + c)

    def remote(src, dst, send, recv, to):
        return pltpu.make_async_remote_copy(
            src_ref=src, dst_ref=dst, send_sem=send, recv_sem=recv, device_id=to, device_id_type=MESH
        )

    def arrived(ref, recv, name="wait"):
        with jax.named_scope(name):
            remote(ref, ref, s_in.at[0], recv, partner).wait_recv()

    def left(ref, send):
        remote(ref, ref, send, s_in.at[0], partner).wait_send()

    barrier = pltpu.get_barrier_semaphore()
    peers = [partner]
    for j in (1, 2, 3):
        peers += [x_peer(j)]
        peers += [(sp, 2 * ((y + j) % 4) + core) for core in (0, 1)]
        peers += [(4 * ((z + j) % 4) + x, 2 * y + core) for core in (0, 1)]
    for peer in peers:
        pl.semaphore_signal(barrier, inc=1, device_id=peer, device_id_type=MESH)

    pairs = [(q_hbm, q), (go_hbm, go), (ao_hbm, ao), (lse_hbm, lse), (lat_hbm, lat), (kw_hbm, kw), (vw_hbm, vw), (rope_hbm, rope)]
    loads = [pltpu.make_async_copy(src, dst, s_in.at[i]) for i, (src, dst) in enumerate(pairs)]
    for load in loads:
        load.start()

    dk[...] = jnp.zeros_like(dk)
    dv[...] = jnp.zeros_like(dv)
    for s in (0, 1):
        kv[s, ONES_AT : ONES_AT + 16] = ones_rows(0)
        kv[s, ONES_AT + 16 : VALUE_AT] = ones_rows(3)

    with jax.named_scope("inputs"):
        for load in loads:
            load.wait()
    with jax.named_scope("barrier"):
        pl.semaphore_wait(barrier, len(peers))

    def to_head(e, src, dst, send, recv):
        head_z = 2 * c + e
        own = (head_z == z) & (core_of_z == c)
        copy = remote(src, dst, send, recv, (4 * head_z + x, 2 * y + core_of_z))
        return own, copy, pltpu.make_async_copy(src, dst, recv)

    def start_to_head(args):
        own, copy, local = to_head(*args)

        @pl.when(own)
        def _():
            local.start()

        @pl.when(jnp.logical_not(own))
        def _():
            copy.start()

    def sent_to_head(args):
        own, copy, _ = to_head(*args)

        @pl.when(jnp.logical_not(own))
        def _():
            copy.wait_send()

    def half(ref, b, h):
        return ref.at[b, :, pl.ds(HALF * h, HALF)]

    pack_args = [
        (e, half(pk, e, h), half(qb, sp, h), s_pk.at[e, h], r_q.at[sp, h]) for h in (0, 1) for e in (0, 1)
    ]
    key_args = [
        (e, kts.at[e], kv.at[slot_of_z, pl.ds(0, HEAD)], s_kt.at[e], r_kt.at[slot_of_z]) for e in (0, 1)
    ]
    value_args = [
        (e, vts.at[e], kv.at[slot_of_z, pl.ds(VALUE_AT, VDIM)], s_v.at[e], r_v.at[slot_of_z]) for e in (0, 1)
    ]

    latent_args = [(e, lat, lt.at[slot_of_z], s_lt.at[e], r_lt.at[slot_of_z]) for e in (0, 1)]

    def send_queries():
        qt = q[...].T
        got = go[...].T
        aot = ao[...].T
        for e in (0, 1):
            grad = got[e * VDIM : (e + 1) * VDIM]
            delta = jnp.sum(
                grad.astype(F32) * aot[e * VDIM : (e + 1) * VDIM].astype(F32), axis=0, keepdims=True
            )
            pk[e, 0:LSE_AT] = qt[e * HEAD : (e + 1) * HEAD]
            pk[e, LSE_AT:GRAD_AT] = six_rows(lse[e : e + 1, :] * (-1.0 / SCALE), -delta)
            pk[e, GRAD_AT:PACK] = grad
        for args in pack_args:
            start_to_head(args)

    def send_keys():
        keys = dot(lat[...], kw[...]).astype(BF16).T
        for e in (0, 1):
            kts[e, 0:NOPE] = keys[e * NOPE : (e + 1) * NOPE]
            kts[e, NOPE:HEAD] = rope[...]
            start_to_head(key_args[e])
        values = dot(lat[...], vw[...]).astype(BF16).T
        for e in (0, 1):
            vts[e] = values[e * VDIM : (e + 1) * VDIM]
            start_to_head(value_args[e])

    @pl.when(z < 2)
    def _():
        send_keys()
        send_queries()

    @pl.when(z >= 2)
    def _():
        send_queries()
        send_keys()

    def weight_copy(kind, dy, p):
        at = 2 * ((y + dy) % 4) + c
        to = (y_peer(1), y_peer(3), partner)[kind]
        return remote(wt.at[at, p], wt.at[at, p], s_wt.at[0], r_wt.at[3 if kind == 2 else 2 if dy else p], to)

    def send_weight(*args):
        copy = weight_copy(*args)
        copy.start()

    def take_weights(p):
        arrived(wt.at[0], r_wt.at[p], "wait_weights")
        for dy in (1, 3):
            send_weight(2, dy, p)
        send_weight(p, 3 - 2 * p, p)

    for p, weights in ((0, kw), (1, vw)):
        wt[tp, p] = weights[...].T
        for kind in (0, 1, 2):
            send_weight(kind, 0, p)

    def zero(b, _):
        dq[b] = jnp.zeros((HEAD, ROWS), F32)
        return 0

    lax.fori_loop(0, 16, zero, 0)

    def step(t):
        near = t < 4
        far = t >= 12
        mid = jnp.logical_not(near | far)
        pair = t % 2
        slot = 1 - jnp.where(mid, (t - 4) // 4, (t % 4) // 2)
        other = jnp.where(mid, ((t - 4) // 2) % 2, pair)
        dx = jnp.where(near, 0, jnp.where(far, 2, jnp.where(pair == 0, 3, 1)))
        core = jnp.where(other == 0, c, 1 - c)
        block = 4 * key_z(core, slot) + (x + dx) % 4
        return block, dx, other, slot

    def forwards(t, h):
        b, dx, other, slot = step(t)
        block = half(qb, b, h)
        mine = other == 0
        plus = mine & ((dx == 0) | ((dx == 3) & (slot == 0)))
        minus = mine & ((dx == 0) | ((dx == 1) & (slot == 1)))
        return [
            (plus, remote(block, block, s_fw.at[0], r_q.at[b, h], x_peer(1))),
            (minus, remote(block, block, s_fw.at[1], r_q.at[b, h], x_peer(3))),
            (mine, remote(block, block, s_fw.at[2], r_q.at[b, h], partner)),
        ]

    def take(t):
        b = step(t)[0]
        for h in (0, 1):
            arrived(half(qb, b, h), r_q.at[b, h], "wait_query")
            for holds, copy in forwards(t, h):

                @pl.when(holds)
                def _():
                    copy.start()

    def tile(b, s, masked):
        raw = dot(kaug[s], qb[b, 0:GRAD_AT]) * (SCALE * LOG2E)
        if masked:
            key_row = lax.broadcasted_iota(jnp.int32, (ROWS, ROWS), 0)
            query_row = lax.broadcasted_iota(jnp.int32, (ROWS, ROWS), 1)
            raw = jnp.where(key_row <= query_row, raw, -1e30)
        probs = jnp.exp2(raw)
        diff = dot(vaug[s], qb[b, LSE_AT:PACK])
        grads = (probs * diff).astype(BF16)
        dv[s] += dot_nt(probs.astype(BF16), qb[b, GRAD_AT:PACK])
        dk[s] += dot_nt(grads, qb[b, 0:LSE_AT])
        dq[b] += dot(kv[s, 0:HEAD], grads)

    def to_partner(i):
        return remote(dqs.at[i], dqr.at[i], s_d.at[0], r_d.at[i], partner)

    def share(t):
        b, dx, other, slot = step(t)

        @pl.when(other == 1)
        def _():
            i = 2 * dx + slot
            dqs[i] = dq[b].astype(BF16)
            to_partner(i).start()

    def own_block(s):
        return 4 * key_z(c, s) + x

    def take_keys(s):
        arrived(kv.at[s, pl.ds(0, HEAD)], r_kt.at[s], "wait_keys")
        arrived(kv.at[s, pl.ds(VALUE_AT, VDIM)], r_v.at[s], "wait_values")
        kaug[s] = kv[s, 0:GRAD_AT].T
        vaug[s] = kv[s, GRAD_AT:KEY_PACK].T

    def tiles(t):
        b = step(t)[0]

        def pair(s, _):
            @pl.when(b > own_block(s))
            def _():
                tile(b, s, False)

            return 0

        with jax.named_scope("pair"):
            lax.fori_loop(0, 2, pair, 0)

    def early(t, _):
        @pl.when(t > 0)
        def _():
            take(t)

        with jax.named_scope("early"):
            tile(step(t)[0], 0, False)
        return 0

    def diagonal(s, _):
        tile(own_block(s), s, True)
        return 0

    def later(t, _):
        take(t)

        @pl.when(t == 5)
        def _():
            take_weights(0)

        @pl.when(t == 8)
        def _():
            take_weights(1)

        tiles(t)
        share(t)
        return 0

    def piece(s, j):
        i = (4 * c + y + j) % 8
        token_z = key_z(c, s)
        to = (4 * token_z + x, 2 * (i % 4) + i // 4)
        src, dst = gs.at[s, i], gf.at[4 * y + z]
        return (
            (token_z == z) if j == 0 else None,
            remote(src, dst, s_g.at[s], r_g.at[y], to),
            pltpu.make_async_copy(src, dst, r_g.at[y]),
        )

    def by_piece(s, j, local_op, remote_op):
        own, copy, local = piece(s, j)
        if own is None:
            remote_op(copy)
            return

        @pl.when(own)
        def _():
            local_op(local)

        @pl.when(jnp.logical_not(own))
        def _():
            remote_op(copy)

    def send_grads(s):
        gs[s, :, 0:CHUNK] = (dk[s, :, 0:NOPE] * SCALE).astype(BF16).reshape(8, CHUNK, NOPE)
        gs[s, :, CHUNK : 2 * CHUNK] = dv[s].astype(BF16).reshape(8, CHUNK, VDIM)
        ropes = (dk[s, :, NOPE:HEAD] * SCALE).astype(BF16).reshape(8, 2, 32, ROPE)
        gs[s, :, 2 * CHUNK : PIECE] = jnp.concatenate([ropes[:, 0], ropes[:, 1]], axis=2)
        for j in range(8):
            by_piece(s, j, lambda local: local.start(), lambda copy: copy.start())

    def to_owner(s, src, dst, send, recv):
        token_z = key_z(c, s)
        own = (token_z == z) & (z // 2 == c)
        copy = remote(src, dst, send, recv, (4 * token_z + x, 2 * y + z // 2))
        return own, copy, pltpu.make_async_copy(src, dst, recv)

    def start_to_owner(args):
        own, copy, local = to_owner(*args)

        @pl.when(own)
        def _():
            local.start()

        @pl.when(jnp.logical_not(own))
        def _():
            copy.start()

    def sent_to_owner(args):
        own, copy, _ = to_owner(*args)

        @pl.when(jnp.logical_not(own))
        def _():
            copy.wait_send()

    e_mine = z % 2
    back = []

    def add_share(dx, s):
        i = 2 * dx + s
        arrived(dqr.at[i], r_d.at[i], "wait_share")
        b = 4 * key_z(c, s) + (x + dx) % 4
        return dq[b] + dqr[i].astype(F32)

    def send_x(i, value, dst, recv, to):
        xs[i] = value.astype(BF16)
        copy = remote(xs.at[i], dst, s_x.at[0], recv, to)
        copy.start()

    def to_hbm(i):
        pltpu.make_async_copy(ag.at[i], ag_out.at[i], s_out.at[2]).start()

    take(0)
    take_keys(0)
    lax.fori_loop(0, 2, early, 0)
    for args in latent_args:
        start_to_head(args)
    take(2)
    take_keys(1)
    with jax.named_scope("diagonal"):
        lax.fori_loop(0, 2, diagonal, 0)

    @pl.when(step(1)[0] > own_block(1))
    def _():
        tile(step(1)[0], 1, False)

    share(1)
    lax.fori_loop(3, 14, later, 0)

    send_grads(1)
    send_x(1, add_share(2, 1), rel.at[1], r_rel.at[1], x_peer(1))
    send_x(2, add_share(3, 1), fin.at[1, 1], r_fin.at[1], x_peer(3))
    send_x(3, add_share(1, 0), fin.at[0, 0], r_fin.at[0], x_peer(1))
    lax.fori_loop(14, 16, later, 0)
    send_grads(0)
    send_x(0, add_share(2, 0), rel.at[0], r_rel.at[0], x_peer(3))

    arrived(wt.at[0], r_wt.at[2], "wait_weights")
    for p in (0, 1):
        send_weight(2, 2, p)

    for args in pack_args + key_args + value_args + latent_args:
        sent_to_head(args)

    left(qb.at[pl.ds(0, 3)], s_fw.at[0])
    left(qb.at[pl.ds(0, 3)], s_fw.at[1])
    left(qb.at[pl.ds(0, 8)], s_fw.at[2])
    left(dqs, s_d.at[0])

    def relay_plus():
        value = add_share(1, 1)
        arrived(rel.at[1], r_rel.at[1], "wait_relay")
        send_x(5, value + rel[1].astype(F32), fin.at[1, 0], r_fin.at[1], x_peer(1))

    def relay_minus():
        value = add_share(3, 0)
        arrived(rel.at[0], r_rel.at[0], "wait_relay")
        send_x(4, value + rel[0].astype(F32), fin.at[0, 1], r_fin.at[0], x_peer(3))

    relay_plus()
    relay_minus()

    arrived(wt.at[pl.ds(0, 4)], r_wt.at[3], "wait_weights")
    latent = jnp.zeros((CHUNK, LATENT), F32)
    ropes = jnp.zeros((32, 2 * ROPE), F32)
    for j in (0, 1, 3, 2):
        yj = (y + j) % 4
        arrived(gf.at[pl.ds(4 * yj, 4)], r_g.at[yj], "wait_grads")
        for u in range(4):
            ropes += gf[4 * yj + u, 2 * CHUNK : PIECE].astype(F32)
        for core in (0, 1):
            first, second = 4 * yj + 2 * core, 4 * yj + 2 * core + 1
            for p in (0, 1):
                rows = slice(p * CHUNK, (p + 1) * CHUNK)
                grads = jnp.concatenate([gf[first, rows], gf[second, rows]], axis=1)
                latent += dot(grads, wt[2 * yj + core, p])
    mine = 4 * c + y
    for i in range(8):
        ag[mine, CHUNK * i : CHUNK * (i + 1)] = latent[:, 128 * i : 128 * (i + 1)].astype(BF16)
    ag[mine, 8 * CHUNK : DONE] = ropes.astype(BF16)
    for j in (2, 1, 3):
        remote(ag.at[mine], ag.at[mine], s_ag.at[0], r_ag.at[mine], y_peer(j)).start()
    remote(ag.at[mine], ag.at[mine], s_ag.at[0], r_ag.at[mine], partner).start()
    to_hbm(mine)

    for s in (0, 1):
        arrived(lt.at[s], r_lt.at[s], "wait_latent")
    weight = dot(gs[0, :, CHUNK : 2 * CHUNK].reshape(ROWS, VDIM).T, lt[0])
    weight += dot(gs[1, :, CHUNK : 2 * CHUNK].reshape(ROWS, VDIM).T, lt[1])
    for core in (0, 1):
        dwh[core] = weight[:, 512 * core : 512 * (core + 1)].astype(BF16).T
    to_half = remote(dwh.at[1 - c], dwhr, s_wh.at[0], r_wh.at[0], partner)
    to_half.start()

    arrived(dwhr, r_wh.at[0], "wait_weight")
    weight = (dwh[c].astype(F32) + dwhr[...].astype(F32)).astype(BF16)
    for i in range(8):
        dwx[i % 4, i // 4] = weight[64 * i : 64 * (i + 1)]
    for j in (2, 1, 3):
        xj = (x + j) % 4
        copy = remote(dwx.at[xj], dwxr.at[x], s_wx.at[0], r_wx.at[0], x_peer(j))
        copy.start()

    for s in (0, 1):
        home = add_share(0, s)
        arrived(fin.at[s], r_fin.at[s], "wait_home")
        home += fin[s, 0].astype(F32) + fin[s, 1].astype(F32)
        dqh[s] = (home * SCALE).astype(BF16)
        args = (s, dqh.at[s], dqf.at[e_mine], s_h.at[s], r_h.at[e_mine])
        start_to_owner(args)
        back.append(args)

    weight = dwx[x].astype(F32)
    arrived(dwxr.at[pl.ds(0, 3)], r_wx.at[0], "wait_weight")
    for j in (1, 3, 2):
        weight += dwxr[(x + j) % 4].astype(F32)
    dwz[...] = weight.astype(BF16)

    def weight_home(i):
        row_z = 2 * c + i
        own = (row_z == z) & (z // 2 == c)
        src, dst = dwz.at[i], dwf.at[z % 2]
        copy = remote(src, dst, s_wz.at[i], r_wz.at[z % 2], (4 * row_z + x, 2 * y + z // 2))
        return own, copy, pltpu.make_async_copy(src, dst, r_wz.at[z % 2])

    for i in (0, 1):
        own, copy, local = weight_home(i)

        @pl.when(own)
        def _():
            local.start()

        @pl.when(jnp.logical_not(own))
        def _():
            copy.start()

    for s in (0, 1):
        own = key_z(c, s) == z

        @pl.when(own)
        def _():
            left(gs.at[s, pl.ds(0, 7)], s_g.at[s])

        @pl.when(jnp.logical_not(own))
        def _():
            left(gs.at[s], s_g.at[s])

    left(wt.at[pl.ds(0, 7)], s_wt.at[0])
    left(xs, s_x.at[0])
    left(dwx.at[pl.ds(0, 3)], s_wx.at[0])

    for j in (1, 3, 2):
        i = 4 * c + (y + j) % 4
        arrived(ag.at[i], r_ag.at[i], "wait_chunk")
        remote(ag.at[i], ag.at[i], s_ag.at[0], r_ag.at[i], partner).start()
        to_hbm(i)

    for e in (0, 1):
        arrived(dwf.at[e], r_wz.at[e], "wait_weight")
        dwo[:, e * VDIM : (e + 1) * VDIM] = dwf[e].astype(F32)
    for e in (0, 1):
        arrived(dqf.at[e], r_h.at[e], "wait_queries")
    dqo[...] = jnp.concatenate([dqf[0], dqf[1]], axis=0).T
    stores = [pltpu.make_async_copy(dqo, dq_out, s_out.at[0]), pltpu.make_async_copy(dwo, dw_out, s_out.at[1])]
    for store in stores:
        store.start()
    for i in (0, 1):
        own, copy, _ = weight_home(i)

        @pl.when(jnp.logical_not(own))
        def _():
            copy.wait_send()

    for args in back:
        sent_to_owner(args)
    for j in (0, 1, 3, 2):
        i = 4 * (1 - c) + (y + j) % 4
        arrived(ag.at[i], r_ag.at[i], "wait_other_chunk")
        to_hbm(i)

    with jax.named_scope("last"):
        to_half.wait_send()
        left(ag.at[pl.ds(0, 7)], s_ag.at[0])
        for store in stores:
            store.wait()
        pltpu.make_async_copy(ag, ag_out, s_out.at[2]).wait()


def finish(ag_hbm, dq_hbm, dw_hbm, dlat_hbm, drope_hbm, dq_out, dw_out, ag, dq, dw, dlat, drope, s_in, s_out):
    loads = [pltpu.make_async_copy(ag_hbm.at[i], ag.at[i], s_in.at[i]) for i in range(8)]
    loads += [pltpu.make_async_copy(dq_hbm, dq, s_in.at[8]), pltpu.make_async_copy(dw_hbm, dw, s_in.at[9])]
    for load in loads:
        load.start()
    stores = []
    for i in range(8):
        loads[i].wait()
        rows = pl.ds(CHUNK * i, CHUNK)
        for j in range(8):
            dlat[rows, 128 * j : 128 * (j + 1)] = ag[i, CHUNK * j : CHUNK * (j + 1)].astype(F32)
        stores.append(pltpu.make_async_copy(dlat.at[rows], dlat_hbm.at[rows], s_out.at[i]))
        stores[-1].start()
    for i, src, dst in ((8, dq, dq_out), (9, dw, dw_out)):
        loads[i].wait()
        stores.append(pltpu.make_async_copy(src, dst, s_out.at[i]))
        stores[-1].start()
    ropes = []
    for i in range(8):
        pairs = ag[i, 8 * CHUNK : DONE].T.astype(F32)
        ropes += [pairs[0:ROPE], pairs[ROPE : 2 * ROPE]]
    drope[...] = jnp.concatenate(ropes, axis=1)
    stores.append(pltpu.make_async_copy(drope, drope_hbm, s_out.at[10]))
    stores[-1].start()
    for store in stores:
        store.wait()


def per_device(q, lat, rope, kw, vw, lse, ao, go):
    vmem = pl.BlockSpec(memory_space=pltpu.VMEM)
    anywhere = pl.BlockSpec(memory_space=pl.ANY)

    def buf(*shape, dtype=BF16):
        return pltpu.VMEM(shape, dtype)

    def sem(*shape):
        return pltpu.SemaphoreType.DMA(shape)

    scratch = [
        buf(ROWS, 2 * HEAD), buf(ROWS, LATENT), buf(ROPE, ROWS), buf(LATENT, 256), buf(LATENT, 256),
        buf(2, ROWS, dtype=F32), buf(ROWS, 256), buf(ROWS, 256),
        buf(16, PACK, ROWS), buf(2, PACK, ROWS), buf(2, HEAD, ROWS), buf(2, VDIM, ROWS),
        buf(2, KEY_PACK, ROWS), buf(2, ROWS, GRAD_AT), buf(2, ROWS, KEY_PACK - GRAD_AT),
        buf(2, ROWS, HEAD, dtype=F32), buf(2, ROWS, VDIM, dtype=F32), buf(16, HEAD, ROWS, dtype=F32),
        buf(8, HEAD, ROWS), buf(8, HEAD, ROWS), buf(6, HEAD, ROWS), buf(2, HEAD, ROWS), buf(2, 2, HEAD, ROWS),
        buf(2, HEAD, ROWS), buf(2, HEAD, ROWS), buf(2, 8, PIECE, 128), buf(16, PIECE, 128),
        buf(2, ROWS, LATENT), buf(8, 2, 256, LATENT),
        buf(2, 512, VDIM), buf(512, VDIM), buf(4, 2, 64, VDIM), buf(4, 2, 64, VDIM), buf(2, 64, VDIM), buf(2, 64, VDIM),
        buf(8, DONE, 128), buf(ROWS, 2 * HEAD), buf(64, 256, dtype=F32),
        sem(8), sem(2, 2), sem(2), sem(2), sem(16, 2), sem(2), sem(2), sem(3), sem(1), sem(8), sem(1), sem(2),
        sem(2), sem(2), sem(2), sem(2), sem(4),
        sem(2), sem(2), sem(1), sem(4), sem(1), sem(8), sem(1), sem(1), sem(1), sem(1), sem(2), sem(2), sem(3),
    ]
    ag, dq, dw = pl.pallas_call(
        kernel,
        in_specs=[anywhere] * 8,
        out_specs=[anywhere] * 3,
        out_shape=[
            jax.ShapeDtypeStruct((8, DONE, 128), BF16),
            jax.ShapeDtypeStruct((ROWS, 2 * HEAD), BF16),
            jax.ShapeDtypeStruct((64, 256), F32),
        ],
        scratch_shapes=scratch,
        compiler_params=pltpu.CompilerParams(
            collective_id=0, has_side_effects=True, vmem_limit_bytes=58000 * 1024
        ),
        name="latent_attention_backward",
    )(q, lat, rope.T, kw, vw, lse, ao, go)
    dlat, drope, dq, dw = pl.pallas_call(
        finish,
        in_specs=[anywhere] * 3,
        out_specs=[anywhere] * 4,
        out_shape=[
            jax.ShapeDtypeStruct((ROWS, LATENT), F32),
            jax.ShapeDtypeStruct((ROPE, ROWS), F32),
            jax.ShapeDtypeStruct((ROWS, 2 * HEAD), BF16),
            jax.ShapeDtypeStruct((64, 256), F32),
        ],
        scratch_shapes=[
            buf(8, DONE, 128), buf(ROWS, 2 * HEAD), buf(64, 256, dtype=F32),
            buf(ROWS, LATENT, dtype=F32), buf(ROPE, ROWS, dtype=F32), sem(10), sem(11),
        ],
        compiler_params=pltpu.CompilerParams(vmem_limit_bytes=58000 * 1024),
        name="finish",
    )(ag, dq, dw)
    return dq, dlat, drope.T, dw


def solution(mesh):
    placed = (
        P("sp", "tp"),
        P("sp", None),
        P("sp", None),
        P(None, "tp"),
        P(None, "tp"),
        P("tp", "sp"),
        P("sp", "tp"),
        P("sp", "tp"),
    )
    return jax.shard_map(
        per_device,
        mesh=mesh,
        in_specs=placed,
        out_specs=(P("sp", "tp"), P("sp", None), P("sp", None), P("sp", "tp")),
        check_vma=False,
    )
```

time: 83.2 us -> 72.2 us (0.87)
  Pallas kernels: 82.4 us -> 70.7 us
    pallas_call x2, Pallas kernels: 82.4 us -> 70.7 us  [the longest x1 68.1 us: per_device(): pl.pallas_call(kernel, in_specs=[anywhere] * 8, out_specs=[anywhere] * 3,...]
where the time goes in v1:
time: 72.2 us; the launch traced here: 71.3 us
  Pallas kernels  70.7 us (98%)
    pallas_call x1, Pallas kernels, per_device(): pl.pallas_call(kernel, in_specs=[anywhere] * 8, out_specs=[anywhere] * 3,...  68.1 us
    pallas_call x1, Pallas kernels, per_device(): pl.pallas_call(finish, in_specs=[anywhere] * 3, out_specs=[anywhere] * 4,...  2.6 us

profile of v1, /device:TPU:1, one launch (start us, length us, event | category | flops | bytes accessed | tf_op | source)
XLA Modules:
  0.0 71.3 jit_solution(17094195962973889847)
XLA Ops:
  0.6 68.1 %latent_attention_backward.1 = (bf16[8,544,128]{2,1,0:T(8,128)(2,1)}, bf16[512,384]{1,0:T(8,128)(2,1)}, f32[64,256]{1,0:T(8,128)}) custom-call(bf16[512,384]{1,0:T(8,128)(2,1)} %q_hbm.1, bf16[512,1024]{1,0:T(8,128)(2,1)} %lat_hbm.1, bf16[64,512]{1,0:T(8,128)(2,1)} %bitcast.2, bf16[1024,256]{1,0:T(8,128)(2,1)} %kw_hbm.1, bf16[1024,256]{1,0:T(8,128)(2,1)} %vw_hbm.1, ...), custom_call_target="tpu_custom_call" | custom-call | tf_op jit(solution)/shard_map/latent_attention_backward/pallas_call | solution.py:635
  68.7 2.6 %finish.1 = (f32[512,1024]{1,0:T(8,128)}, f32[64,512]{1,0:T(8,128)}, bf16[512,384]{1,0:T(8,128)(2,1)}, f32[64,256]{1,0:T(8,128)}) custom-call(bf16[8,544,128]{2,1,0:T(8,128)(2,1)} %get-tuple-element.11.ag_hbm, bf16[512,384]{1,0:T(8,128)(2,1)} %get-tuple-element.12.dq_hbm, f32[64,256]{1,0:T(8,128)} %get-tuple-element.13.dw_hbm), custom_call_target="tpu_custom_call" | custom-call | tf_op jit(solution)/shard_map/finish/pallas_call | solution.py:650

commit v2 on v1

--- a/solution.py
+++ b/solution.py
@@ -102,22 +102,25 @@
     for peer in peers:
         pl.semaphore_signal(barrier, inc=1, device_id=peer, device_id_type=MESH)
 
-    pairs = [(q_hbm, q), (go_hbm, go), (ao_hbm, ao), (lse_hbm, lse), (lat_hbm, lat), (kw_hbm, kw), (vw_hbm, vw), (rope_hbm, rope)]
-    loads = [pltpu.make_async_copy(src, dst, s_in.at[i]) for i, (src, dst) in enumerate(pairs)]
-    for load in loads:
-        load.start()
+    def load(i):
+        pairs = ((q_hbm, q), (go_hbm, go), (ao_hbm, ao), (lse_hbm, lse), (lat_hbm, lat), (kw_hbm, kw), (rope_hbm, rope), (vw_hbm, vw))
+        return pltpu.make_async_copy(*pairs[i], s_in.at[i])
+
+    @pl.when(z < 2)
+    def _():
+        for i in (4, 5, 6, 7, 0, 1, 2, 3):
+            load(i).start()
+
+    @pl.when(z >= 2)
+    def _():
+        for i in range(8):
+            load(i).start()
 
     dk[...] = jnp.zeros_like(dk)
     dv[...] = jnp.zeros_like(dv)
     for s in (0, 1):
         kv[s, ONES_AT : ONES_AT + 16] = ones_rows(0)
         kv[s, ONES_AT + 16 : VALUE_AT] = ones_rows(3)
-
-    with jax.named_scope("inputs"):
-        for load in loads:
-            load.wait()
-    with jax.named_scope("barrier"):
-        pl.semaphore_wait(barrier, len(peers))
 
     def to_head(e, src, dst, send, recv):
         head_z = 2 * c + e
@@ -158,7 +161,9 @@
 
     latent_args = [(e, lat, lt.at[slot_of_z], s_lt.at[e], r_lt.at[slot_of_z]) for e in (0, 1)]
 
-    def send_queries():
+    def pack_queries():
+        for i in range(4):
+            load(i).wait()
         qt = q[...].T
         got = go[...].T
         aot = ao[...].T
@@ -170,29 +175,25 @@
             pk[e, 0:LSE_AT] = qt[e * HEAD : (e + 1) * HEAD]
             pk[e, LSE_AT:GRAD_AT] = six_rows(lse[e : e + 1, :] * (-1.0 / SCALE), -delta)
             pk[e, GRAD_AT:PACK] = grad
-        for args in pack_args:
-            start_to_head(args)
-
-    def send_keys():
+
+    def pack_keys():
+        for i in range(4, 8):
+            load(i).wait()
         keys = dot(lat[...], kw[...]).astype(BF16).T
         for e in (0, 1):
             kts[e, 0:NOPE] = keys[e * NOPE : (e + 1) * NOPE]
             kts[e, NOPE:HEAD] = rope[...]
-            start_to_head(key_args[e])
         values = dot(lat[...], vw[...]).astype(BF16).T
         for e in (0, 1):
             vts[e] = values[e * VDIM : (e + 1) * VDIM]
-            start_to_head(value_args[e])
-
-    @pl.when(z < 2)
-    def _():
-        send_keys()
-        send_queries()
-
-    @pl.when(z >= 2)
-    def _():
-        send_queries()
-        send_keys()
+
+    def send_queries():
+        for args in pack_args:
+            start_to_head(args)
+
+    def send_keys():
+        for args in key_args + value_args:
+            start_to_head(args)
 
     def weight_copy(kind, dy, p):
         at = 2 * ((y + dy) % 4) + c
@@ -209,10 +210,37 @@
             send_weight(2, dy, p)
         send_weight(p, 3 - 2 * p, p)
 
-    for p, weights in ((0, kw), (1, vw)):
-        wt[tp, p] = weights[...].T
+    def send_own_weights(p):
+        wt[tp, p] = (kw, vw)[p][...].T
         for kind in (0, 1, 2):
             send_weight(kind, 0, p)
+
+    @pl.when(z < 2)
+    def _():
+        pack_keys()
+
+    @pl.when(z >= 2)
+    def _():
+        pack_queries()
+
+    with jax.named_scope("barrier"):
+        pl.semaphore_wait(barrier, len(peers))
+
+    @pl.when(z < 2)
+    def _():
+        send_keys()
+        send_own_weights(0)
+        pack_queries()
+        send_queries()
+
+    @pl.when(z >= 2)
+    def _():
+        send_queries()
+        pack_keys()
+        send_keys()
+        send_own_weights(0)
+
+    send_own_weights(1)
 
     def zero(b, _):
         dq[b] = jnp.zeros((HEAD, ROWS), F32)
@@ -273,11 +301,9 @@
     def share(t):
         b, dx, other, slot = step(t)
 
-        @pl.when(other == 1)
-        def _():
-            i = 2 * dx + slot
-            dqs[i] = dq[b].astype(BF16)
-            to_partner(i).start()
+        i = 2 * dx + slot
+        dqs[i] = dq[b].astype(BF16)
+        to_partner(i).start()
 
     def own_block(s):
         return 4 * key_z(c, s) + x
@@ -288,18 +314,24 @@
         kaug[s] = kv[s, 0:GRAD_AT].T
         vaug[s] = kv[s, GRAD_AT:KEY_PACK].T
 
-    def tiles(t):
-        b = step(t)[0]
-
-        def pair(s, _):
-            @pl.when(b > own_block(s))
+    def both_tiles(b):
+        probs = [jnp.exp2(dot(kaug[s], qb[b, 0:GRAD_AT]) * (SCALE * LOG2E)) for s in (0, 1)]
+        grads = [(probs[s] * dot(vaug[s], qb[b, LSE_AT:PACK])).astype(BF16) for s in (0, 1)]
+        for s in (0, 1):
+            dv[s] += dot_nt(probs[s].astype(BF16), qb[b, GRAD_AT:PACK])
+            dk[s] += dot_nt(grads[s], qb[b, 0:LSE_AT])
+        dq[b] += dot(kv[0, 0:HEAD], grads[0]) + dot(kv[1, 0:HEAD], grads[1])
+
+    def tiles(b):
+        with jax.named_scope("pair"):
+
+            @pl.when(b > own_block(1))
             def _():
-                tile(b, s, False)
-
-            return 0
-
-        with jax.named_scope("pair"):
-            lax.fori_loop(0, 2, pair, 0)
+                both_tiles(b)
+
+            @pl.when((b > own_block(0)) & (b < own_block(1)))
+            def _():
+                tile(b, 0, False)
 
     def early(t, _):
         @pl.when(t > 0)
@@ -314,19 +346,79 @@
         tile(own_block(s), s, True)
         return 0
 
-    def later(t, _):
-        take(t)
-
-        @pl.when(t == 5)
+    def later(p, _):
+        far = p >= 6
+        even = jnp.logical_not(far) & (p % 2 == 0)
+        odd = jnp.logical_not(far) & (p % 2 == 1)
+        slot = step(2 * p)[3]
+
+        @pl.when(even)
+        def _():
+            for h in (0, 1):
+                for i, back_slot in ((0, 0), (1, 1)):
+                    b = step(2 * p + i)[0]
+                    block = half(qb, b, h)
+                    arrived(block, r_q.at[b, h], "wait_query")
+
+                    @pl.when(slot == back_slot)
+                    def _():
+                        remote(block, block, s_fw.at[i], r_q.at[b, h], x_peer(1 + 2 * i)).start()
+
+                    remote(block, block, s_fw.at[2], r_q.at[b, h], partner).start()
+
+        @pl.when(odd)
+        def _():
+            for i in (0, 1):
+                b = step(2 * p + i)[0]
+                for h in (0, 1):
+                    arrived(half(qb, b, h), r_q.at[b, h], "wait_query")
+
+        @pl.when(far)
+        def _():
+            b = step(2 * p)[0]
+            for h in (0, 1):
+                block = half(qb, b, h)
+                arrived(block, r_q.at[b, h], "wait_query")
+                remote(block, block, s_fw.at[2], r_q.at[b, h], partner).start()
+
+        @pl.when(p == 2)
         def _():
             take_weights(0)
 
-        @pl.when(t == 8)
+        @pl.when(p == 4)
         def _():
             take_weights(1)
 
-        tiles(t)
-        share(t)
+        def member(i, _):
+            b = step(2 * p + i)[0]
+
+            @pl.when(far & (i == 1))
+            def _():
+                for h in (0, 1):
+                    arrived(half(qb, b, h), r_q.at[b, h], "wait_query")
+
+            tiles(b)
+            return 0
+
+        lax.fori_loop(0, 2, member, 0)
+
+        @pl.when(odd)
+        def _():
+            share(2 * p)
+
+        @pl.when(odd | far)
+        def _():
+            share(2 * p + 1)
+
+        return 0
+
+    def rest(i, _):
+        b = step(1 + 2 * i)[0]
+
+        @pl.when(b > own_block(1 - i))
+        def _():
+            tile(b, 1 - i, False)
+
         return 0
 
     def piece(s, j):
@@ -413,18 +505,17 @@
     with jax.named_scope("diagonal"):
         lax.fori_loop(0, 2, diagonal, 0)
 
-    @pl.when(step(1)[0] > own_block(1))
-    def _():
-        tile(step(1)[0], 1, False)
-
+    take(3)
+    lax.fori_loop(0, 2, rest, 0)
     share(1)
-    lax.fori_loop(3, 14, later, 0)
+    share(3)
+    lax.fori_loop(2, 7, later, 0)
 
     send_grads(1)
     send_x(1, add_share(2, 1), rel.at[1], r_rel.at[1], x_peer(1))
     send_x(2, add_share(3, 1), fin.at[1, 1], r_fin.at[1], x_peer(3))
     send_x(3, add_share(1, 0), fin.at[0, 0], r_fin.at[0], x_peer(1))
-    lax.fori_loop(14, 16, later, 0)
+    lax.fori_loop(7, 8, later, 0)
     send_grads(0)
     send_x(0, add_share(2, 0), rel.at[0], r_rel.at[0], x_peer(3))
 

time: 72.2 us -> 70.6 us (0.978)
  Pallas kernels: 70.7 us -> 69.6 us
    pallas_call x1, Pallas kernels: 68.1 us -> 67 us  [per_device(): pl.pallas_call(kernel, in_specs=[anywhere] * 8, out_specs=[anywhere] * 3,...]
where the time goes in v2:
time: 70.6 us; the launch traced here: 70.4 us
  Pallas kernels  69.6 us (99%)
  between operations  0.8 us (1%)
    pallas_call x1, Pallas kernels, per_device(): pl.pallas_call(kernel, in_specs=[anywhere] * 8, out_specs=[anywhere] * 3,...  67 us
    pallas_call x1, Pallas kernels, per_device(): pl.pallas_call(finish, in_specs=[anywhere] * 3, out_specs=[anywhere] * 4,...  2.6 us

profile of v2, /device:TPU:1, one launch (start us, length us, event | category | flops | bytes accessed | tf_op | source)
XLA Modules:
  0.0 70.4 jit_solution(3678650589041380006)
XLA Ops:
  0.6 67.0 %latent_attention_backward.1 = (bf16[8,544,128]{2,1,0:T(8,128)(2,1)}, bf16[512,384]{1,0:T(8,128)(2,1)}, f32[64,256]{1,0:T(8,128)}) custom-call(bf16[512,384]{1,0:T(8,128)(2,1)} %q_hbm.1, bf16[512,1024]{1,0:T(8,128)(2,1)} %lat_hbm.1, bf16[64,512]{1,0:T(8,128)(2,1)} %bitcast.2, bf16[1024,256]{1,0:T(8,128)(2,1)} %kw_hbm.1, bf16[1024,256]{1,0:T(8,128)(2,1)} %vw_hbm.1, ...), custom_call_target="tpu_custom_call" | custom-call | tf_op jit(solution)/shard_map/latent_attention_backward/pallas_call | solution.py:726
  67.7 2.6 %finish.1 = (f32[512,1024]{1,0:T(8,128)}, f32[64,512]{1,0:T(8,128)}, bf16[512,384]{1,0:T(8,128)(2,1)}, f32[64,256]{1,0:T(8,128)}) custom-call(bf16[8,544,128]{2,1,0:T(8,128)(2,1)} %get-tuple-element.11.ag_hbm, bf16[512,384]{1,0:T(8,128)(2,1)} %get-tuple-element.12.dq_hbm, f32[64,256]{1,0:T(8,128)} %get-tuple-element.13.dw_hbm), custom_call_target="tpu_custom_call" | custom-call | tf_op jit(solution)/shard_map/finish/pallas_call | solution.py:741

commit v3 on v2

--- a/solution.py
+++ b/solution.py
@@ -237,10 +237,16 @@
     def _():
         send_queries()
         pack_keys()
+        send_own_weights(0)
+        send_own_weights(1)
         send_keys()
-        send_own_weights(0)
-
-    send_own_weights(1)
+
+    @pl.when(z < 2)
+    def _():
+        send_own_weights(1)
+
+    for args in latent_args:
+        start_to_head(args)
 
     def zero(b, _):
         dq[b] = jnp.zeros((HEAD, ROWS), F32)
@@ -498,8 +504,6 @@
     take(0)
     take_keys(0)
     lax.fori_loop(0, 2, early, 0)
-    for args in latent_args:
-        start_to_head(args)
     take(2)
     take_keys(1)
     with jax.named_scope("diagonal"):
@@ -564,7 +568,7 @@
     ag[mine, 8 * CHUNK : DONE] = ropes.astype(BF16)
     for j in (2, 1, 3):
         remote(ag.at[mine], ag.at[mine], s_ag.at[0], r_ag.at[mine], y_peer(j)).start()
-    remote(ag.at[mine], ag.at[mine], s_ag.at[0], r_ag.at[mine], partner).start()
+    remote(ag.at[mine], ag_out.at[mine], s_ag.at[0], r_ag.at[mine], partner).start()
     to_hbm(mine)
 
     for s in (0, 1):
@@ -636,7 +640,7 @@
     for j in (1, 3, 2):
         i = 4 * c + (y + j) % 4
         arrived(ag.at[i], r_ag.at[i], "wait_chunk")
-        remote(ag.at[i], ag.at[i], s_ag.at[0], r_ag.at[i], partner).start()
+        remote(ag.at[i], ag_out.at[i], s_ag.at[0], r_ag.at[i], partner).start()
         to_hbm(i)
 
     for e in (0, 1):
@@ -659,15 +663,14 @@
         sent_to_owner(args)
     for j in (0, 1, 3, 2):
         i = 4 * (1 - c) + (y + j) % 4
-        arrived(ag.at[i], r_ag.at[i], "wait_other_chunk")
-        to_hbm(i)
+        arrived(ag_out.at[i], r_ag.at[i], "wait_other_chunk")
 
     with jax.named_scope("last"):
         to_half.wait_send()
         left(ag.at[pl.ds(0, 7)], s_ag.at[0])
         for store in stores:
             store.wait()
-        pltpu.make_async_copy(ag, ag_out, s_out.at[2]).wait()
+        pltpu.make_async_copy(ag.at[pl.ds(0, 4)], ag_out.at[pl.ds(0, 4)], s_out.at[2]).wait()
 
 
 def finish(ag_hbm, dq_hbm, dw_hbm, dlat_hbm, drope_hbm, dq_out, dw_out, ag, dq, dw, dlat, drope, s_in, s_out):

time: 70.6 us -> 70.3 us (level)
  no operation moved by 1% of the time
where the time goes in v3:
time: 70.3 us; the launch traced here: 70.2 us
  Pallas kernels  69.4 us (99%)
  between operations  0.8 us (1%)
    pallas_call x1, Pallas kernels, per_device(): pl.pallas_call(kernel, in_specs=[anywhere] * 8, out_specs=[anywhere] * 3,...  66.8 us
    pallas_call x1, Pallas kernels, per_device(): pl.pallas_call(finish, in_specs=[anywhere] * 3, out_specs=[anywhere] * 4,...  2.6 us

profile of v3, /device:TPU:1, one launch (start us, length us, event | category | flops | bytes accessed | tf_op | source)
XLA Modules:
  0.0 70.2 jit_solution(10524216045536494883)
XLA Ops:
  0.6 66.8 %latent_attention_backward.1 = (bf16[8,544,128]{2,1,0:T(8,128)(2,1)}, bf16[512,384]{1,0:T(8,128)(2,1)}, f32[64,256]{1,0:T(8,128)}) custom-call(bf16[512,384]{1,0:T(8,128)(2,1)} %q_hbm.1, bf16[512,1024]{1,0:T(8,128)(2,1)} %lat_hbm.1, bf16[64,512]{1,0:T(8,128)(2,1)} %bitcast.2, bf16[1024,256]{1,0:T(8,128)(2,1)} %kw_hbm.1, bf16[1024,256]{1,0:T(8,128)(2,1)} %vw_hbm.1, ...), custom_call_target="tpu_custom_call" | custom-call | tf_op jit(solution)/shard_map/latent_attention_backward/pallas_call | solution.py:729
  67.4 2.6 %finish.1 = (f32[512,1024]{1,0:T(8,128)}, f32[64,512]{1,0:T(8,128)}, bf16[512,384]{1,0:T(8,128)(2,1)}, f32[64,256]{1,0:T(8,128)}) custom-call(bf16[8,544,128]{2,1,0:T(8,128)(2,1)} %get-tuple-element.11.ag_hbm, bf16[512,384]{1,0:T(8,128)(2,1)} %get-tuple-element.12.dq_hbm, f32[64,256]{1,0:T(8,128)} %get-tuple-element.13.dw_hbm), custom_call_target="tpu_custom_call" | custom-call | tf_op jit(solution)/shard_map/finish/pallas_call | solution.py:744

commit v4 on v3

--- a/solution.py
+++ b/solution.py
@@ -457,7 +457,7 @@
         gs[s, :, CHUNK : 2 * CHUNK] = dv[s].astype(BF16).reshape(8, CHUNK, VDIM)
         ropes = (dk[s, :, NOPE:HEAD] * SCALE).astype(BF16).reshape(8, 2, 32, ROPE)
         gs[s, :, 2 * CHUNK : PIECE] = jnp.concatenate([ropes[:, 0], ropes[:, 1]], axis=2)
-        for j in range(8):
+        for j in (2, 6, 1, 5, 3, 7, 4, 0):
             by_piece(s, j, lambda local: local.start(), lambda copy: copy.start())
 
     def to_owner(s, src, dst, send, recv):

time: 70.3 us -> 70.7 us (level)
  no operation moved by 1% of the time
where the time goes in v4:
time: 70.7 us; the launch traced here: 70.5 us
  Pallas kernels  69.7 us (99%)
  between operations  0.8 us (1%)
    pallas_call x1, Pallas kernels, per_device(): pl.pallas_call(kernel, in_specs=[anywhere] * 8, out_specs=[anywhere] * 3,...  67.1 us
    pallas_call x1, Pallas kernels, per_device(): pl.pallas_call(finish, in_specs=[anywhere] * 3, out_specs=[anywhere] * 4,...  2.6 us

profile of v4, /device:TPU:1, one launch (start us, length us, event | category | flops | bytes accessed | tf_op | source)
XLA Modules:
  0.0 70.5 jit_solution(4459590851246672108)
XLA Ops:
  0.6 67.1 %latent_attention_backward.1 = (bf16[8,544,128]{2,1,0:T(8,128)(2,1)}, bf16[512,384]{1,0:T(8,128)(2,1)}, f32[64,256]{1,0:T(8,128)}) custom-call(bf16[512,384]{1,0:T(8,128)(2,1)} %q_hbm.1, bf16[512,1024]{1,0:T(8,128)(2,1)} %lat_hbm.1, bf16[64,512]{1,0:T(8,128)(2,1)} %bitcast.2, bf16[1024,256]{1,0:T(8,128)(2,1)} %kw_hbm.1, bf16[1024,256]{1,0:T(8,128)(2,1)} %vw_hbm.1, ...), custom_call_target="tpu_custom_call" | custom-call | tf_op jit(solution)/shard_map/latent_attention_backward/pallas_call | solution.py:729
  67.7 2.6 %finish.1 = (f32[512,1024]{1,0:T(8,128)}, f32[64,512]{1,0:T(8,128)}, bf16[512,384]{1,0:T(8,128)(2,1)}, f32[64,256]{1,0:T(8,128)}) custom-call(bf16[8,544,128]{2,1,0:T(8,128)(2,1)} %get-tuple-element.11.ag_hbm, bf16[512,384]{1,0:T(8,128)(2,1)} %get-tuple-element.12.dq_hbm, f32[64,256]{1,0:T(8,128)} %get-tuple-element.13.dw_hbm), custom_call_target="tpu_custom_call" | custom-call | tf_op jit(solution)/shard_map/finish/pallas_call | solution.py:744

commit v5 on v3

--- a/solution.py
+++ b/solution.py
@@ -348,10 +348,6 @@
             tile(step(t)[0], 0, False)
         return 0
 
-    def diagonal(s, _):
-        tile(own_block(s), s, True)
-        return 0
-
     def later(p, _):
         far = p >= 6
         even = jnp.logical_not(far) & (p % 2 == 0)
@@ -418,12 +414,23 @@
 
         return 0
 
-    def rest(i, _):
-        b = step(1 + 2 * i)[0]
-
-        @pl.when(b > own_block(1 - i))
-        def _():
-            tile(b, 1 - i, False)
+    def own_tiles(s, _):
+        @pl.when(s == 1)
+        def _():
+            take_keys(1)
+
+        with jax.named_scope("diagonal"):
+            tile(own_block(s), s, True)
+
+        @pl.when(s == 0)
+        def _():
+            take(3)
+
+        b = step(3 - 2 * s)[0]
+
+        @pl.when(b > own_block(s))
+        def _():
+            tile(b, s, False)
 
         return 0
 
@@ -505,12 +512,7 @@
     take_keys(0)
     lax.fori_loop(0, 2, early, 0)
     take(2)
-    take_keys(1)
-    with jax.named_scope("diagonal"):
-        lax.fori_loop(0, 2, diagonal, 0)
-
-    take(3)
-    lax.fori_loop(0, 2, rest, 0)
+    lax.fori_loop(0, 2, own_tiles, 0)
     share(1)
     share(3)
     lax.fori_loop(2, 7, later, 0)
@@ -674,20 +676,22 @@
 
 
 def finish(ag_hbm, dq_hbm, dw_hbm, dlat_hbm, drope_hbm, dq_out, dw_out, ag, dq, dw, dlat, drope, s_in, s_out):
-    loads = [pltpu.make_async_copy(ag_hbm.at[i], ag.at[i], s_in.at[i]) for i in range(8)]
-    loads += [pltpu.make_async_copy(dq_hbm, dq, s_in.at[8]), pltpu.make_async_copy(dw_hbm, dw, s_in.at[9])]
+    pairs_of = [pl.ds(2 * i, 2) for i in range(4)]
+    loads = [pltpu.make_async_copy(ag_hbm.at[two], ag.at[two], s_in.at[i]) for i, two in enumerate(pairs_of)]
+    loads += [pltpu.make_async_copy(dq_hbm, dq, s_in.at[4]), pltpu.make_async_copy(dw_hbm, dw, s_in.at[5])]
     for load in loads:
         load.start()
     stores = []
     for i in range(8):
-        loads[i].wait()
+        if i % 2 == 0:
+            loads[i // 2].wait()
         rows = pl.ds(CHUNK * i, CHUNK)
         for j in range(8):
             dlat[rows, 128 * j : 128 * (j + 1)] = ag[i, CHUNK * j : CHUNK * (j + 1)].astype(F32)
-        stores.append(pltpu.make_async_copy(dlat.at[rows], dlat_hbm.at[rows], s_out.at[i]))
-        stores[-1].start()
-    for i, src, dst in ((8, dq, dq_out), (9, dw, dw_out)):
-        loads[i].wait()
+        pltpu.make_async_copy(dlat.at[rows], dlat_hbm.at[rows], s_out.at[0]).start()
+    stores.append(pltpu.make_async_copy(dlat, dlat_hbm, s_out.at[0]))
+    for i, src, dst in ((1, dq, dq_out), (2, dw, dw_out)):
+        loads[3 + i].wait()
         stores.append(pltpu.make_async_copy(src, dst, s_out.at[i]))
         stores[-1].start()
     ropes = []
@@ -695,7 +699,7 @@
         pairs = ag[i, 8 * CHUNK : DONE].T.astype(F32)
         ropes += [pairs[0:ROPE], pairs[ROPE : 2 * ROPE]]
     drope[...] = jnp.concatenate(ropes, axis=1)
-    stores.append(pltpu.make_async_copy(drope, drope_hbm, s_out.at[10]))
+    stores.append(pltpu.make_async_copy(drope, drope_hbm, s_out.at[3]))
     stores[-1].start()
     for store in stores:
         store.wait()
@@ -753,7 +757,7 @@
         ],
         scratch_shapes=[
             buf(8, DONE, 128), buf(ROWS, 2 * HEAD), buf(64, 256, dtype=F32),
-            buf(ROWS, LATENT, dtype=F32), buf(ROPE, ROWS, dtype=F32), sem(10), sem(11),
+            buf(ROWS, LATENT, dtype=F32), buf(ROPE, ROWS, dtype=F32), sem(6), sem(4),
         ],
         compiler_params=pltpu.CompilerParams(vmem_limit_bytes=58000 * 1024),
         name="finish",

time: 70.3 us -> 70.5 us (level)
  no operation moved by 1% of the time
where the time goes in v5:
time: 70.5 us; the launch traced here: 70.3 us
  Pallas kernels  69.5 us (99%)
  between operations  0.8 us (1%)
    pallas_call x1, Pallas kernels, per_device(): pl.pallas_call(kernel, in_specs=[anywhere] * 8, out_specs=[anywhere] * 3,...  66.9 us
    pallas_call x1, Pallas kernels, per_device(): pl.pallas_call(finish, in_specs=[anywhere] * 3, out_specs=[anywhere] * 4,...  2.56 us

profile of v5, /device:TPU:1, one launch (start us, length us, event | category | flops | bytes accessed | tf_op | source)
XLA Modules:
  0.0 70.3 jit_solution(15234768971734629579)
XLA Ops:
  0.6 66.9 %latent_attention_backward.1 = (bf16[8,544,128]{2,1,0:T(8,128)(2,1)}, bf16[512,384]{1,0:T(8,128)(2,1)}, f32[64,256]{1,0:T(8,128)}) custom-call(bf16[512,384]{1,0:T(8,128)(2,1)} %q_hbm.1, bf16[512,1024]{1,0:T(8,128)(2,1)} %lat_hbm.1, bf16[64,512]{1,0:T(8,128)(2,1)} %bitcast.2, bf16[1024,256]{1,0:T(8,128)(2,1)} %kw_hbm.1, bf16[1024,256]{1,0:T(8,128)(2,1)} %vw_hbm.1, ...), custom_call_target="tpu_custom_call" | custom-call | tf_op jit(solution)/shard_map/latent_attention_backward/pallas_call | solution.py:733
  67.6 2.6 %finish.1 = (f32[512,1024]{1,0:T(8,128)}, f32[64,512]{1,0:T(8,128)}, bf16[512,384]{1,0:T(8,128)(2,1)}, f32[64,256]{1,0:T(8,128)}) custom-call(bf16[8,544,128]{2,1,0:T(8,128)(2,1)} %get-tuple-element.11.ag_hbm, bf16[512,384]{1,0:T(8,128)(2,1)} %get-tuple-element.12.dq_hbm, f32[64,256]{1,0:T(8,128)} %get-tuple-element.13.dw_hbm), custom_call_target="tpu_custom_call" | custom-call | tf_op jit(solution)/shard_map/finish/pallas_call | solution.py:748
